TPU v7x, 32 devices: a whole 2x2x4 slice. The times are simulated.
32 devices in a mesh: grp: 2 (over y), fs: 4 (over z), tp: 4 (over x, core).
Axes of the slice: x: 2, y: 2, z: 4, core: 2. Of those that a mesh axis runs over, the one named last changes fastest.
Arguments:
- hidden_activations: bfloat16 [2048, 6144], P('tp', ('grp', 'fs')), parts along dimension 1, may hold values from -6 to 6
- attention_rescaling_factors: float32 [2048], replicated, may hold values from 0.1 to 1.9
- feature_rescaling_factors: float32 [2048], replicated, may hold values from 0.1 to 1.9
- request_matrix: float32 [2048, 2048], P('fs', 'tp'), may hold values from -0.125 to 0.125
- request_matrix_multipliers: float32 [2048], P('tp'), may hold values from 0.1 to 1.9
- lookup_matrix: float32 [2048, 2048], P('fs', 'tp'), may hold values from -0.125 to 0.125
- lookup_matrix_multipliers: float32 [2048], P('tp'), may hold values from 0.1 to 1.9
- content_matrix: float32 [2048, 4096], P('fs', 'tp'), may hold values from -0.125 to 0.125
- content_matrix_multipliers: float32 [4096], P('tp'), may hold values from 0.1 to 1.9
- valve_matrix: float32 [2048, 4096], P('fs', 'tp'), may hold values from -0.125 to 0.125
- valve_matrix_multipliers: float32 [4096], P('tp'), may hold values from 0.1 to 1.9
- result_matrix: float32 [4096, 2048], P('tp', 'fs'), may hold values from -0.09375 to 0.09375
- result_matrix_multipliers: float32 [2048], P('fs'), may hold values from 0.1 to 1.9
- expanding_matrix: float32 [2048, 8192], P('fs', 'tp'), may hold values from -0.125 to 0.125
- expand_matrix_multipliers: float32 [8192], P('tp'), may hold values from 0.1 to 1.9
- shrinking_matrix: float32 [8192, 2048], P('tp', 'fs'), may hold values from -0.0625 to 0.0625
- shrink_matrix_multipliers: float32 [2048], P('fs'), may hold values from 0.1 to 1.9
- attention_fading_logarithm: float32 [8], P('tp'), may hold values from -1 to 0
- spike_fading_logarithm: float32 [8, 6144], P('tp', ('grp', 'fs')), parts along dimension 1, may hold values from -1 to 0, as said below
Outputs:
- out_stream: bfloat16 [2048, 6144], P('tp', ('grp', 'fs')), parts along dimension 1
There are 2 independent parts, one for each index of `grp`. A program takes and returns all parts, laid end to end along the dimension named above; an argument that names none is the same for every part. Nothing has to cross between parts.
Inputs may be any that keep to these rules, and one draw needn't show every extreme that they name: `spike_fading_logarithm`: log decay added to the head's own.
All inputs are finite; a program needn't handle non-finite values.
Results may differ from a plain program's by a relative error of at most 0.019.
Values may be sent and summed in bfloat16 or wider, within the bound.
A program may use at most 128 MiB of HBM per device.

v0:
```python
import jax
import jax.numpy as jnp
from jax import lax
from jax.sharding import PartitionSpec as P

DK = 256
DV = 512
BLOCK_POSITIONS = 128
epsilon = 1e-06


def as_sent(value):

    def short(part):
        return part.astype(jnp.bfloat16) if part.dtype == jnp.float32 else part

    return jax.tree.map(short, value)


def rms_norm(matrix, norm_gain):
    values = matrix.astype(jnp.float32)
    factor = lax.rsqrt(jnp.mean(values * values, axis=0, keepdims=True) + epsilon)
    return (values * factor * norm_gain[:, None]).astype(jnp.bfloat16)


def project(normed, weight):
    return lax.dot_general(
        normed, weight, (((0,), (0,)), ((), ())), preferred_element_type=jnp.float32
    )


def collect_features(matrix):
    return lax.all_gather(matrix, "tp", axis=0, tiled=True)


def retain(query, keys, values, fading_logarithm_speed):
    length = query.shape[2]
    causal = jnp.arange(length)[:, None] >= jnp.arange(length)[None, :]

    def advance(memory, inputs):
        query_blk, key_blk, value_blk, rate_blk = inputs
        running = jnp.cumsum(rate_blk, axis=-1)
        closing = running[:, -1:]
        spread = jnp.where(causal, running[:, :, None] - running[:, None, :], 0.0)
        decays = jnp.where(causal, jnp.exp(spread), 0.0)
        scores = (
            jnp.einsum("gid,gjd->gij", query_blk, key_blk, preferred_element_type=jnp.float32)
            * decays
        )
        weights = scores.astype(jnp.bfloat16)
        within = jnp.einsum("gij,gjv->giv", weights, value_blk, preferred_element_type=jnp.float32)
        state_copy = memory.astype(jnp.bfloat16)
        carried = (
            jnp.einsum("gid,gdv->giv", query_blk, state_copy, preferred_element_type=jnp.float32)
            * jnp.exp(running)[:, :, None]
        )
        faded_keys = (key_blk.astype(jnp.float32) * jnp.exp(closing - running)[:, :, None]).astype(
            jnp.bfloat16
        )
        memory = memory * jnp.exp(closing)[:, :, None] + jnp.einsum(
            "gjd,gjv->gdv", faded_keys, value_blk, preferred_element_type=jnp.float32
        )
        return (memory, within + carried)

    initial = jnp.zeros((query.shape[0], query.shape[3], values.shape[3]), jnp.float32)
    stacked = tuple(
        (jnp.swapaxes(member, 0, 1) for member in (query, keys, values, fading_logarithm_speed))
    )
    _, outputs = lax.scan(advance, initial, stacked)
    return jnp.swapaxes(outputs, 0, 1)


def to_heads(matrix, width):
    token_inputs = matrix.shape[0]
    split = matrix.reshape(
        token_inputs // BLOCK_POSITIONS, BLOCK_POSITIONS, matrix.shape[1] // width, width
    )
    return jnp.transpose(split, (2, 0, 1, 3))


def group_norm(retained):
    center = jnp.mean(retained, axis=-1, keepdims=True)
    offset = retained - center
    variance = jnp.mean(offset * offset, axis=-1, keepdims=True)
    return offset * lax.rsqrt(variance + epsilon)


def squared_relu(summed, column_scale):
    rising = jax.nn.relu(summed * column_scale)
    return (rising * rising).astype(jnp.bfloat16)


def local(
    hidden_activations,
    attention_rescaling_factors,
    feature_rescaling_factors,
    request_matrix,
    request_matrix_multipliers,
    lookup_matrix,
    lookup_matrix_multipliers,
    content_matrix,
    content_matrix_multipliers,
    valve_matrix,
    valve_matrix_multipliers,
    result_matrix,
    result_matrix_multipliers,
    expanding_matrix,
    expand_matrix_multipliers,
    shrinking_matrix,
    shrink_matrix_multipliers,
    attention_fading_logarithm,
    spike_fading_logarithm,
):
    out_scales, down_scales = (
        lax.all_gather(result_matrix_multipliers, "fs", axis=0, tiled=True),
        lax.all_gather(shrink_matrix_multipliers, "fs", axis=0, tiled=True),
    )
    normed = rms_norm(collect_features(hidden_activations), attention_rescaling_factors)
    token_inputs = normed.shape[1]
    matrices = (request_matrix, lookup_matrix, content_matrix, valve_matrix)
    pieces = jax.tree.map(
        lambda part: lax.all_gather(part, "fs", axis=0, tiled=True),
        as_sent(tuple((matrix.astype(jnp.bfloat16) for matrix in matrices))),
    )
    picked = normed
    query_sum, key_sum, value_sum, gate_sum = tuple(
        (project(picked, segment) for segment in pieces)
    )
    query = (query_sum * request_matrix_multipliers).astype(jnp.bfloat16)
    keys = (key_sum * lookup_matrix_multipliers * DK ** (-0.5)).astype(jnp.bfloat16)
    values = (value_sum * content_matrix_multipliers).astype(jnp.bfloat16)
    gate = gate_sum * valve_matrix_multipliers
    shard_heads = attention_fading_logarithm.shape[0]
    fading_logarithm_speed = (attention_fading_logarithm[:, None] + spike_fading_logarithm).reshape(
        shard_heads, token_inputs // BLOCK_POSITIONS, BLOCK_POSITIONS
    )
    retained = retain(
        to_heads(query, DK), to_heads(keys, DK), to_heads(values, DV), fading_logarithm_speed
    )
    retained = jnp.transpose(retained, (1, 2, 0, 3)).reshape(token_inputs, shard_heads, DV)
    heads_out = (
        group_norm(retained).reshape(token_inputs, shard_heads * DV) * jax.nn.silu(gate)
    ).astype(jnp.bfloat16)
    out_whole = lax.all_gather(result_matrix.astype(jnp.bfloat16), "fs", axis=1, tiled=True)
    factors = out_scales
    update = lax.psum_scatter(
        (
            lax.dot_general(
                out_whole, heads_out, (((0,), (1,)), ((), ())), preferred_element_type=jnp.float32
            )
            * factors[:, None]
        ).astype(jnp.bfloat16),
        "tp",
        scatter_dimension=0,
        tiled=True,
    ).astype(jnp.float32)
    middle = (hidden_activations.astype(jnp.float32) + update).astype(jnp.bfloat16)
    normed_mlp = rms_norm(collect_features(middle), feature_rescaling_factors)
    picked = normed_mlp
    up_sum = project(
        picked, lax.all_gather(expanding_matrix.astype(jnp.bfloat16), "fs", axis=0, tiled=True)
    )
    hidden = squared_relu(up_sum, expand_matrix_multipliers)
    factors = down_scales
    terms = (
        lax.dot_general(
            lax.all_gather(shrinking_matrix.astype(jnp.bfloat16), "fs", axis=1, tiled=True),
            hidden,
            (((0,), (1,)), ((), ())),
            preferred_element_type=jnp.float32,
        )
        * factors[:, None]
    )
    lowered = lax.psum_scatter(
        terms.astype(jnp.bfloat16), "tp", scatter_dimension=0, tiled=True
    ).astype(jnp.float32)
    return (middle.astype(jnp.float32) + lowered).astype(jnp.bfloat16)


def solution(mesh):
    placed = (
        P("tp", ("grp", "fs")),
        P(),
        P(),
        P("fs", "tp"),
        P("tp"),
        P("fs", "tp"),
        P("tp"),
        P("fs", "tp"),
        P("tp"),
        P("fs", "tp"),
        P("tp"),
        P("tp", "fs"),
        P("fs"),
        P("fs", "tp"),
        P("tp"),
        P("tp", "fs"),
        P("fs"),
        P("tp"),
        P("tp", ("grp", "fs")),
    )
    return jax.shard_map(
        local, mesh=mesh, in_specs=placed, out_specs=P("tp", ("grp", "fs")), check_vma=False
    )
```

profile of v0, /device:TPU:0, one launch (start us, length us, event | category | flops | bytes accessed | tf_op | source)
XLA Modules:
  0.0 824.8 jit_solution(7764887072463206395)
XLA Ops:
  11.8 2.8 convert_element_type.99
  16.1 14.3 %all-gather = f32[4,1,512]{2,1,0:T(1,128)} all-gather(f32[1,1,512]{2,1,0:T(1,128)S(1)} %bitcast.91), channel_id=1, replica_groups=mesh['grp'=2,'fs'=4,'tp'=4] {'fs'}, dimensions={0}, use_global_device_ids=true | all-gather | bytes 10240 | tf_op jit(solution)/shard_map/all_gather | solution.py:115
  30.5 9.7 %all-gather.12.cloned.1.call-done = bf16[2048,768]{1,0:T(8,128)(2,1)} async-done(((bf16[512,768]{1,0:T(8,128)(2,1)}), bf16[2048,768]{1,0:T(8,128)(2,1)}) %all-gather.12.cloned.1.call-update) | async-done | bytes 3145744 | tf_op jit(solution)/shard_map/all_gather | solution.py:33
  42.8 44.7 %all-gather.14.cloned.1.call-done = bf16[2048,512]{1,0:T(8,128)(2,1)} async-done(((bf16[512,512]{1,0:T(8,128)(2,1)}), bf16[2048,512]{1,0:T(8,128)(2,1)}) %all-gather.14.cloned.1.call-update) | async-done | bytes 2097168 | tf_op jit(solution)/shard_map/all_gather | solution.py:122
  87.4 4.5 multiply_convert_fusion.8
  92.1 41.4 %all-gather.18.cloned.1.call-done = bf16[2048,512]{1,0:T(8,128)(2,1)} async-done(((bf16[512,512]{1,0:T(8,128)(2,1)}), bf16[2048,512]{1,0:T(8,128)(2,1)}) %all-gather.18.cloned.1.call-update) | async-done | bytes 2097168 | tf_op jit(solution)/shard_map/all_gather | solution.py:122
  133.5 4.5 multiply_convert_fusion.7
  139.6 74.9 %all-gather.16.cloned.1.call-done = bf16[2048,1024]{1,0:T(8,128)(2,1)} async-done(((bf16[512,1024]{1,0:T(8,128)(2,1)}), bf16[2048,1024]{1,0:T(8,128)(2,1)}) %all-gather.16.cloned.1.call-update) | async-done | bytes 4194320 | tf_op jit(solution)/shard_map/all_gather | solution.py:122
  214.5 6.9 multiply_convert_fusion.6
  221.4 2.6 reshape.102
  225.8 31.8 %while.14 = (s32[]{:T(128)}, f32[2,256,512]{2,1,0:T(8,128)S(1)}, f32[6,2,128,512]{3,2,1,0:T(8,128)}, f32[6,2,128]{2,1,0:T(2,128)S(1)}, bf16[6,2,128,256]{3,2,1,0...) while((s32[]{:T(128)}, f32[2,256,512]{2,1,0:T(8,128)S(1)}, ...), condition=%wide.region_3.4_spmd.clone.clone, body=%wide.region_1.3_spmd.clone.clone.sunk | while | flops 186269696 | bytes 5815448 | solution.py:69
  273.3 21.9 %all-gather.20.cloned.1.call-done = bf16[2048,1024]{1,0:T(8,128)(2,1)} async-done(((bf16[512,1024]{1,0:T(8,128)(2,1)}), bf16[2048,1024]{1,0:T(8,128)(2,1)}) %all-gather.20.cloned.1.call-update) | async-done | bytes 4194320 | tf_op jit(solution)/shard_map/all_gather | solution.py:122
  295.2 80.7 %all-gather.22.cloned.1.call-done = bf16[1024,2048]{1,0:T(8,128)(2,1)} async-done(((bf16[1024,512]{1,0:T(8,128)(2,1)}), bf16[1024,2048]{1,0:T(8,128)(2,1)}) %all-gather.22.cloned.1.call-update) | async-done | bytes 4194320 | tf_op jit(solution)/shard_map/all_gather | solution.py:144
  375.9 15.5 %fusion.49 = bf16[2048,768]{0,1:T(8,128)(2,1)} fusion(f32[2048]{0:T(1024)S(1)} %bitcast.89, bf16[1024,2048]{1,0:T(8,128)(2,1)} %all-gather.22.cloned.1.call-done, f32[768,1024]{1,0:T(8,128)} %bitcast.86, f32[768,1024]{1,0:T(8,128)} %bitcast.88, f32[768,1024]{1,0:T(8,128)} %bitcast.87, bf16[2048,1024]{1,0:T(8,128)(2,1)} %all-gather.20.cloned.1.call-done, ...), kind=kOutput, calls=%fused_computation.63 | convolution fusion | flops 6458966016 | bytes 24140800 | tf_op jit(solution)/shard_map/dot_general | solution.py:148
  392.8 35.0 %reduce-scatter.3.cloned.1.call-done = bf16[512,768]{0,1:T(8,128)(2,1)} async-done(((bf16[2048,768]{0,1:T(8,128)(2,1)}), bf16[512,768]{0,1:T(8,128)(2,1)}) %reduce-scatter.3.cloned.1.call-update) | async-done | bytes 786448 | tf_op jit(solution)/shard_map/reduce_scatter | solution.py:146
  430.0 3.9 convert_element_type.109
  434.0 3.9 convert_element_type.111
  437.9 12.2 %all-gather.1 = f32[4,1,512]{2,1,0:T(1,128)S(1)} all-gather(f32[1,1,512]{2,1,0:T(1,128)S(1)} %bitcast.92), channel_id=1, replica_groups=mesh['grp'=2,'fs'=4,'tp'=4] {'fs'}, dimensions={0}, use_global_device_ids=true | all-gather | bytes 10240 | tf_op jit(solution)/shard_map/all_gather | solution.py:116
  450.1 8.6 %all-gather.24.cloned.1.call-done = bf16[2048,768]{0,1:T(8,128)(2,1)} async-done(((bf16[512,768]{0,1:T(8,128)(2,1)}), bf16[2048,768]{0,1:T(8,128)(2,1)}) %all-gather.24.cloned.1.call-update) | async-done | bytes 3145744 | tf_op jit(solution)/shard_map/all_gather | solution.py:33
  458.6 2.7 fusion.42
  461.4 148.5 %all-gather.26.cloned.1.call-done = bf16[2048,2048]{1,0:T(8,128)(2,1)} async-done(((bf16[512,2048]{1,0:T(8,128)(2,1)}), bf16[2048,2048]{1,0:T(8,128)(2,1)}) %all-gather.26.cloned.1.call-update) | async-done | bytes 8388624 | tf_op jit(solution)/shard_map/all_gather | solution.py:161
  609.9 149.2 %all-gather.28.cloned.1.call-done = bf16[2048,2048]{1,0:T(8,128)(2,1)} async-done(((bf16[2048,512]{1,0:T(8,128)(2,1)}), bf16[2048,2048]{1,0:T(8,128)(2,1)}) %all-gather.28.cloned.1.call-update) | async-done | bytes 8388624 | tf_op jit(solution)/shard_map/all_gather | solution.py:167
  759.1 20.6 %fusion.48 = bf16[2048,768]{0,1:T(8,128)(2,1)} fusion(f32[2048]{0:T(1024)S(1)} %bitcast.90, bf16[2048,2048]{1,0:T(8,128)(2,1)} %all-gather.28.cloned.1.call-done, bf16[2048,2048]{1,0:T(8,128)(2,1)} %all-gather.26.cloned.1.call-done, bf16[2048,768]{0,1:T(8,128)(2,1)S(1)} %copy-done.3, f32[2048]{0:T(1024)S(1)} %copy-done.17, f32[2048]{0:T(1024)S(1)} %copy-done.18, ...), kind=kOutput, calls=%fused_computation.62 | convolution fusion | flops 12900630528 | bytes 23096320 | tf_op jit(solution)/shard_map/dot_general | solution.py:166
  779.7 36.1 %reduce-scatter.5.cloned.1.call-done = bf16[512,768]{0,1:T(8,128)(2,1)} async-done(((bf16[2048,768]{0,1:T(8,128)(2,1)}), bf16[512,768]{0,1:T(8,128)(2,1)}) %reduce-scatter.5.cloned.1.call-update) | async-done | bytes 786448 | tf_op jit(solution)/shard_map/reduce_scatter | solution.py:174
  (146 shorter events, 66.3 us)
Async XLA Ops:
  6.5 33.6 %all-gather.12.cloned.1.call-start = ((), (), s32[]{:S(2)}) async-start(), calls=%async_computation.2 | async-start | bytes 3932160 | tf_op jit(solution)/shard_map/all_gather | solution.py:33
  7.3 80.2 %all-gather.14.cloned.1.call-start = ((), (), s32[]{:S(2)}) async-start(), calls=%async_computation.3 | async-start | bytes 2621440 | tf_op jit(solution)/shard_map/all_gather | solution.py:122
  9.6 123.9 %all-gather.18.cloned.1.call-start = ((), (), s32[]{:S(2)}) async-start(), calls=%async_computation.5 | async-start | bytes 2621440 | tf_op jit(solution)/shard_map/all_gather | solution.py:122
  10.5 204.0 %all-gather.16.cloned.1.call-start = ((), (), s32[]{:S(2)}) async-start(), calls=%async_computation.4 | async-start | bytes 5242880 | tf_op jit(solution)/shard_map/all_gather | solution.py:122
  11.8 283.4 %all-gather.20.cloned.1.call-start = ((), (), s32[]{:S(2)}) async-start(), calls=%async_computation.6 | async-start | bytes 5242880 | tf_op jit(solution)/shard_map/all_gather | solution.py:122
  14.7 72.7 %copy-start.15 = (f32[2048]{0:T(1024)S(1)}, f32[2048]{0:T(1024)}, u32[]{:S(2)}) copy-start(f32[2048]{0:T(1024)} %param.22) | copy-start | bytes 24580
  14.7 72.7 %copy-start.21 = (f32[512]{0:T(512)S(1)}, f32[512]{0:T(512)}, u32[]{:S(2)}) copy-start(f32[512]{0:T(512)} %param.27) | copy-start | bytes 6148
  14.7 361.1 %all-gather.22.cloned.1.call-start = ((), (), s32[]{:S(2)}) async-start(), calls=%async_computation.7 | async-start | bytes 5242880 | tf_op jit(solution)/shard_map/all_gather | solution.py:144
  16.0 411.7 %reduce-scatter.3.cloned.1.call-start = ((), (), s32[]{:S(2)}) async-start(), calls=%async_computation.8 | async-start | bytes 3932160 | tf_op jit(solution)/shard_map/reduce_scatter | solution.py:146
  42.7 171.8 %copy-start.10 = (f32[768]{0:T(1024)}, f32[768]{0:T(1024)S(1)}, u32[]{:S(2)}) copy-start(f32[768]{0:T(1024)S(1)} %add_rsqrt_fusion.1) | copy-start | bytes 9220
  42.8 90.7 %copy-start.22 = (f32[512]{0:T(512)S(1)}, f32[512]{0:T(512)}, u32[]{:S(2)}) copy-start(f32[512]{0:T(512)} %param.25) | copy-start | bytes 6148
  138.0 76.5 %copy-start.19 = (f32[1024]{0:T(1024)S(1)}, f32[1024]{0:T(1024)}, u32[]{:S(2)}) copy-start(f32[1024]{0:T(1024)} %param.29) | copy-start | bytes 12292
  270.8 105.1 %copy-start.2 = (bf16[2048,768]{1,0:T(8,128)(2,1)S(1)}, bf16[2048,768]{1,0:T(8,128)(2,1)}, u32[]{:S(2)}) copy-start(bf16[2048,768]{1,0:T(8,128)(2,1)} %all-gather.12.cloned.1.call-done) | copy-start | bytes 9437188
  270.8 105.0 %copy-start.8 = (f32[4,1,512]{2,1,0:T(1,128)S(1)}, f32[4,1,512]{2,1,0:T(1,128)}, u32[]{:S(2)}) copy-start(f32[4,1,512]{2,1,0:T(1,128)} %all-gather) | copy-start | bytes 24580
  270.8 105.0 %copy-start.11 = (f32[768]{0:T(1024)S(1)}, f32[768]{0:T(1024)}, u32[]{:S(2)}) copy-start(f32[768]{0:T(1024)} %copy-done.10) | copy-start | bytes 9220
  270.8 105.0 %copy-start.16 = (f32[2048]{0:T(1024)S(1)}, f32[2048]{0:T(1024)}, u32[]{:S(2)}) copy-start(f32[2048]{0:T(1024)} %param.22) | copy-start | bytes 24580
  270.9 105.0 %copy-start.20 = (f32[1024]{0:T(1024)S(1)}, f32[1024]{0:T(1024)}, u32[]{:S(2)}) copy-start(f32[1024]{0:T(1024)} %param.31) | copy-start | bytes 12292
  391.4 67.3 %all-gather.24.cloned.1.call-start = ((), (), s32[]{:S(2)}) async-start(), calls=%async_computation.9 | async-start | bytes 3932160 | tf_op jit(solution)/shard_map/all_gather | solution.py:33
  430.0 179.9 %all-gather.26.cloned.1.call-start = ((), (), s32[]{:S(2)}) async-start(), calls=%async_computation.10 | async-start | bytes 10485760 | tf_op jit(solution)/shard_map/all_gather | solution.py:161
  433.9 325.2 %all-gather.28.cloned.1.call-start = ((), (), s32[]{:S(2)}) async-start(), calls=%async_computation.11 | async-start | bytes 10485760 | tf_op jit(solution)/shard_map/all_gather | solution.py:167
  437.8 321.3 %copy-start.17 = (f32[2048]{0:T(1024)S(1)}, f32[2048]{0:T(1024)}, u32[]{:S(2)}) copy-start(f32[2048]{0:T(1024)} %param.35) | copy-start | bytes 24580
  437.8 321.3 %copy-start.18 = (f32[2048]{0:T(1024)S(1)}, f32[2048]{0:T(1024)}, u32[]{:S(2)}) copy-start(f32[2048]{0:T(1024)} %param.23) | copy-start | bytes 24580
  437.9 377.9 %reduce-scatter.5.cloned.1.call-start = ((), (), s32[]{:S(2)}) async-start(), calls=%async_computation.12 | async-start | bytes 3932160 | tf_op jit(solution)/shard_map/reduce_scatter | solution.py:174
  458.6 300.5 %copy-start.3 = (bf16[2048,768]{0,1:T(8,128)(2,1)S(1)}, bf16[2048,768]{0,1:T(8,128)(2,1)}, u32[]{:S(2)}) copy-start(bf16[2048,768]{0,1:T(8,128)(2,1)} %all-gather.24.cloned.1.call-done) | copy-start | bytes 9437188
  (10 other events, 87.1 us)
Sparse Core Ops, SparseCore 0:
  8.9 31.2 all-gather.11
  41.7 45.6 all-gather.13
  89.0 44.4 all-gather.17
  134.9 79.5 all-gather.15
  215.9 79.2 all-gather.19
  296.6 79.2 all-gather.21
  391.5 36.1 reduce-scatter.2
  430.1 28.5 all-gather.23
  460.2 149.6 all-gather.25
  611.3 147.7 all-gather.27
  779.9 35.8 reduce-scatter.4
where the time goes:
time: 826 us; the launch traced here: 825 us
  waiting for transfers between devices  651 us (79%)
  matrix products  79.9 us (10%)
  other arithmetic  30.3 us (4%)
  blocking collectives  26.4 us (3%)
  local copies, waits for them, and re-layouts  22.6 us (3%)
  between operations  13.5 us (2%)
    all_gather x4, waiting for transfers between devices, local(): lax.all_gather(part, 'fs', axis=0, tiled=True)  183 us
    all_gather x1, waiting for transfers between devices, local(): lax.all_gather(shrinking_matrix.astype(jnp.bfloat16), 'fs', axis=1, tiled...  149 us
    all_gather x1, waiting for transfers between devices, local(): lax.all_gather(expanding_matrix.astype(jnp.bfloat16), 'fs', axis=0, tiled...  148 us
    all_gather x1, waiting for transfers between devices, local(): lax.all_gather(result_matrix.astype(jnp.bfloat16), 'fs', axis=1, tiled=True)  80.7 us
    reduce_scatter x1, waiting for transfers between devices, local(): lax.psum_scatter(terms.astype(jnp.bfloat16), 'tp', scatter_dimension=0, t...  36.1 us
    reduce_scatter x1, waiting for transfers between devices, local(): lax.psum_scatter((lax.dot_general(out_whole, heads_out, (((0,), (1,)), ((...  35 us
    dot_general x1, matrix products, local(): lax.dot_general(lax.all_gather(shrinking_matrix.astype(jnp.bfloat16), 'fs...  20.6 us
    all_gather x2, waiting for transfers between devices, collect_features(): return lax.all_gather(matrix, 'tp', axis=0, tiled=True)  18.2 us
  transfers between devices with their start and end apart: 11, of which 11 were waited for; matrix products, arithmetic and copies ran while one was open for 11% of the time, Pallas kernels for 0%

commit v1 on v0

--- a/solution.py
+++ b/solution.py
@@ -141,7 +141,12 @@
     heads_out = (
         group_norm(retained).reshape(token_inputs, shard_heads * DV) * jax.nn.silu(gate)
     ).astype(jnp.bfloat16)
-    out_whole = lax.all_gather(result_matrix.astype(jnp.bfloat16), "fs", axis=1, tiled=True)
+    out_whole = jnp.concatenate(
+        lax.all_to_all(
+            jnp.stack([result_matrix.astype(jnp.bfloat16)] * lax.axis_size("fs")), "fs", 0, 0
+        ),
+        axis=1,
+    )
     factors = out_scales
     update = lax.psum_scatter(
         (

time: 826 us -> 803 us (0.972)
  waiting for transfers between devices: 651 us -> 503 us
  blocking collectives: 26.4 us -> 144 us
    all_gather x1, blocking collectives: 14.3 us -> 132 us  [local(): lax.all_gather(result_matrix_multipliers, 'fs', axis=0, tiled=True)]
    all_gather x1 -> x0, waiting for transfers between devices: 80.7 us -> none  [local(): lax.all_gather(result_matrix.astype(jnp.bfloat16), 'fs', axis=1, tiled=True)]
    all_gather x4, waiting for transfers between devices: 183 us -> 125 us  [local(): lax.all_gather(part, 'fs', axis=0, tiled=True)]
    all_gather x2, waiting for transfers between devices: 18.2 us -> 8.55 us  [collect_features(): return lax.all_gather(matrix, 'tp', axis=0, tiled=True)]
  transfers between devices with their start and end apart: 11 -> 11, of which waited for: 11 -> 8; matrix products, arithmetic and copies ran while one was open for 11% -> 12% of each run, Pallas kernels for 0% -> 0%
where the time goes in v1:
time: 803 us; the launch traced here: 802 us
  waiting for transfers between devices  503 us (63%)
  blocking collectives  144 us (18%)
  matrix products  79.9 us (10%)
  other arithmetic  29.2 us (4%)
  local copies, waits for them, and re-layouts  25.7 us (3%)
  between operations  13.9 us (2%)
    all_gather x1, waiting for transfers between devices, local(): lax.all_gather(shrinking_matrix.astype(jnp.bfloat16), 'fs', axis=1, tiled...  149 us
    all_gather x1, waiting for transfers between devices, local(): lax.all_gather(expanding_matrix.astype(jnp.bfloat16), 'fs', axis=0, tiled...  148 us
    all_gather x1, blocking collectives, local(): lax.all_gather(result_matrix_multipliers, 'fs', axis=0, tiled=True)  132 us
    all_gather x4, waiting for transfers between devices, local(): lax.all_gather(part, 'fs', axis=0, tiled=True)  125 us
    reduce_scatter x1, waiting for transfers between devices, local(): lax.psum_scatter(terms.astype(jnp.bfloat16), 'tp', scatter_dimension=0, t...  36.1 us
    reduce_scatter x1, waiting for transfers between devices, local(): lax.psum_scatter((lax.dot_general(out_whole, heads_out, (((0,), (1,)), ((...  35 us
    dot_general x1, matrix products, local(): lax.dot_general(lax.all_gather(shrinking_matrix.astype(jnp.bfloat16), 'fs...  20.6 us
  transfers between devices with their start and end apart: 11, of which 8 were waited for; matrix products, arithmetic and copies ran while one was open for 12% of the time, Pallas kernels for 0%

profile of v1, /device:TPU:0, one launch (start us, length us, event | category | flops | bytes accessed | tf_op | source)
XLA Modules:
  0.0 802.4 jit_solution(2741615474646970527)
XLA Ops:
  14.1 2.5 stack.2
  16.6 6.6 all-to-all-start
  24.6 131.5 %all-gather = f32[4,1,512]{2,1,0:T(1,128)} all-gather(f32[1,1,512]{2,1,0:T(1,128)S(1)} %bitcast.94), channel_id=1, replica_groups=mesh['grp'=2,'fs'=4,'tp'=4] {'fs'}, dimensions={0}, use_global_device_ids=true | all-gather | bytes 10240 | tf_op jit(solution)/shard_map/all_gather | solution.py:115
  156.2 2.6 fusion.39
  158.9 4.5 multiply_convert_fusion.8
  163.6 27.8 %all-gather.17.cloned.1.call-done = bf16[2048,512]{1,0:T(8,128)(2,1)} async-done(((bf16[512,512]{1,0:T(8,128)(2,1)}), bf16[2048,512]{1,0:T(8,128)(2,1)}) %all-gather.17.cloned.1.call-update) | async-done | bytes 2097168 | tf_op jit(solution)/shard_map/all_gather | solution.py:122
  191.4 4.5 multiply_convert_fusion.7
  197.5 74.9 %all-gather.15.cloned.1.call-done = bf16[2048,1024]{1,0:T(8,128)(2,1)} async-done(((bf16[512,1024]{1,0:T(8,128)(2,1)}), bf16[2048,1024]{1,0:T(8,128)(2,1)}) %all-gather.15.cloned.1.call-update) | async-done | bytes 4194320 | tf_op jit(solution)/shard_map/all_gather | solution.py:122
  272.4 6.9 multiply_convert_fusion.6
  279.2 2.6 reshape.110
  283.6 31.8 %while.14 = (s32[]{:T(128)}, f32[2,256,512]{2,1,0:T(8,128)S(1)}, f32[6,2,128,512]{3,2,1,0:T(8,128)}, f32[6,2,128]{2,1,0:T(2,128)S(1)}, bf16[6,2,128,256]{3,2,1,0...) while((s32[]{:T(128)}, f32[2,256,512]{2,1,0:T(8,128)S(1)}, ...), condition=%wide.region_3.4_spmd.clone.clone, body=%wide.region_1.3_spmd.clone.clone.sunk | while | flops 186269696 | bytes 5815448 | solution.py:69
  323.8 2.4 copy.48
  331.2 21.9 %all-gather.19.cloned.1.call-done = bf16[2048,1024]{1,0:T(8,128)(2,1)} async-done(((bf16[512,1024]{1,0:T(8,128)(2,1)}), bf16[2048,1024]{1,0:T(8,128)(2,1)}) %all-gather.19.cloned.1.call-update) | async-done | bytes 4194320 | tf_op jit(solution)/shard_map/all_gather | solution.py:122
  353.1 15.4 %fusion.49 = bf16[2048,768]{0,1:T(8,128)(2,1)} fusion(f32[2048]{0:T(1024)S(1)} %bitcast.92, bf16[1024,2048]{0,1:T(8,128)(2,1)} %bitcast.9, f32[768,1024]{1,0:T(8,128)} %bitcast.89, f32[768,1024]{1,0:T(8,128)} %bitcast.91, f32[768,1024]{1,0:T(8,128)} %bitcast.90, bf16[2048,1024]{1,0:T(8,128)(2,1)} %all-gather.19.cloned.1.call-done, f32[1024]{0:T(1024)S(1)} %copy-done.20, ...), kind=kOutput, calls=%fused_computation.63 | convolution fusion | flops 6458966016 | bytes 24140800 | tf_op jit(solution)/shard_map/dot_general | solution.py:153
  369.9 35.0 %reduce-scatter.3.cloned.1.call-done = bf16[512,768]{0,1:T(8,128)(2,1)} async-done(((bf16[2048,768]{0,1:T(8,128)(2,1)}), bf16[512,768]{0,1:T(8,128)(2,1)}) %reduce-scatter.3.cloned.1.call-update) | async-done | bytes 786448 | tf_op jit(solution)/shard_map/reduce_scatter | solution.py:151
  407.2 3.9 convert_element_type.109
  411.1 3.9 convert_element_type.111
  415.1 12.2 %all-gather.1 = f32[4,1,512]{2,1,0:T(1,128)S(1)} all-gather(f32[1,1,512]{2,1,0:T(1,128)S(1)} %bitcast.95), channel_id=1, replica_groups=mesh['grp'=2,'fs'=4,'tp'=4] {'fs'}, dimensions={0}, use_global_device_ids=true | all-gather | bytes 10240 | tf_op jit(solution)/shard_map/all_gather | solution.py:116
  427.2 8.5 %all-gather.21.cloned.1.call-done = bf16[2048,768]{0,1:T(8,128)(2,1)} async-done(((bf16[512,768]{0,1:T(8,128)(2,1)}), bf16[2048,768]{0,1:T(8,128)(2,1)}) %all-gather.21.cloned.1.call-update) | async-done | bytes 3145744 | tf_op jit(solution)/shard_map/all_gather | solution.py:33
  435.8 2.7 fusion.42
  438.5 148.5 %all-gather.23.cloned.1.call-done = bf16[2048,2048]{1,0:T(8,128)(2,1)} async-done(((bf16[512,2048]{1,0:T(8,128)(2,1)}), bf16[2048,2048]{1,0:T(8,128)(2,1)}) %all-gather.23.cloned.1.call-update) | async-done | bytes 8388624 | tf_op jit(solution)/shard_map/all_gather | solution.py:166
  587.0 149.4 %all-gather.25.cloned.1.call-done = bf16[2048,2048]{1,0:T(8,128)(2,1)} async-done(((bf16[2048,512]{1,0:T(8,128)(2,1)}), bf16[2048,2048]{1,0:T(8,128)(2,1)}) %all-gather.25.cloned.1.call-update) | async-done | bytes 8388624 | tf_op jit(solution)/shard_map/all_gather | solution.py:172
  736.4 20.6 %fusion.48 = bf16[2048,768]{0,1:T(8,128)(2,1)} fusion(f32[2048]{0:T(1024)S(1)} %bitcast.93, bf16[2048,2048]{1,0:T(8,128)(2,1)} %all-gather.25.cloned.1.call-done, bf16[2048,2048]{1,0:T(8,128)(2,1)} %all-gather.23.cloned.1.call-done, bf16[2048,768]{0,1:T(8,128)(2,1)S(1)} %copy-done.3, f32[2048]{0:T(1024)S(1)} %copy-done.17, f32[2048]{0:T(1024)S(1)} %copy-done.18, ...), kind=kOutput, calls=%fused_computation.62 | convolution fusion | flops 12900630528 | bytes 23096320 | tf_op jit(solution)/shard_map/dot_general | solution.py:171
  757.0 36.1 %reduce-scatter.5.cloned.1.call-done = bf16[512,768]{0,1:T(8,128)(2,1)} async-done(((bf16[2048,768]{0,1:T(8,128)(2,1)}), bf16[512,768]{0,1:T(8,128)(2,1)}) %reduce-scatter.5.cloned.1.call-update) | async-done | bytes 786448 | tf_op jit(solution)/shard_map/reduce_scatter | solution.py:179
  (147 shorter events, 63.5 us)
Async XLA Ops:
  6.5 149.7 %all-gather.11.cloned.1.call-start = ((), (), s32[]{:S(2)}) async-start(), calls=%async_computation.3 | async-start | bytes 3932160 | tf_op jit(solution)/shard_map/all_gather | solution.py:33
  7.3 151.6 %all-gather.13.cloned.1.call-start = ((), (), s32[]{:S(2)}) async-start(), calls=%async_computation.4 | async-start | bytes 2621440 | tf_op jit(solution)/shard_map/all_gather | solution.py:122
  9.6 181.7 %all-gather.17.cloned.1.call-start = ((), (), s32[]{:S(2)}) async-start(), calls=%async_computation.6 | async-start | bytes 2621440 | tf_op jit(solution)/shard_map/all_gather | solution.py:122
  10.6 261.8 %all-gather.15.cloned.1.call-start = ((), (), s32[]{:S(2)}) async-start(), calls=%async_computation.5 | async-start | bytes 5242880 | tf_op jit(solution)/shard_map/all_gather | solution.py:122
  16.6 314.5 %all-to-all-start = ((bf16[4,1024,512]{1,2,0:T(8,128)(2,1)}), bf16[4,1024,512]{1,2,0:T(8,128)(2,1)}, u32[]{:S(2)}, u32[]{:S(2)}) async-start(bf16[4,1024,512]{1,2,0:T(8,128)(2,1)} %stack.2), calls=%async_computation | async-start | bytes 8388608 | tf_op jit(solution)/shard_map/all_to_all | solution.py:145
  23.3 132.9 %copy-start.9 = (f32[2,768]{1,0:T(2,128)S(1)}, f32[2,768]{1,0:T(2,128)}, u32[]{:S(2)}) copy-start(f32[2,768]{1,0:T(2,128)} %param.39) | copy-start | bytes 18436
  23.3 132.9 %copy-start.14 = (f32[2]{0:T(128)S(1)}, f32[2]{0:T(128)}, u32[]{:S(2)}) copy-start(f32[2]{0:T(128)} %param.38) | copy-start | bytes 28
  23.3 135.6 %copy-start.15 = (f32[2048]{0:T(1024)S(1)}, f32[2048]{0:T(1024)}, u32[]{:S(2)}) copy-start(f32[2048]{0:T(1024)} %param.22) | copy-start | bytes 24580
  23.3 135.6 %copy-start.21 = (f32[512]{0:T(512)S(1)}, f32[512]{0:T(512)}, u32[]{:S(2)}) copy-start(f32[512]{0:T(512)} %param.27) | copy-start | bytes 6148
  23.3 329.7 %all-gather.19.cloned.1.call-start = ((), (), s32[]{:S(2)}) async-start(), calls=%async_computation.7 | async-start | bytes 5242880 | tf_op jit(solution)/shard_map/all_gather | solution.py:122
  24.5 380.4 %reduce-scatter.3.cloned.1.call-start = ((), (), s32[]{:S(2)}) async-start(), calls=%async_computation.8 | async-start | bytes 3932160 | tf_op jit(solution)/shard_map/reduce_scatter | solution.py:151
  158.8 113.5 %copy-start.10 = (f32[768]{0:T(1024)}, f32[768]{0:T(1024)S(1)}, u32[]{:S(2)}) copy-start(f32[768]{0:T(1024)S(1)} %add_rsqrt_fusion.1) | copy-start | bytes 9220
  158.8 32.5 %copy-start.22 = (f32[512]{0:T(512)S(1)}, f32[512]{0:T(512)}, u32[]{:S(2)}) copy-start(f32[512]{0:T(512)} %param.25) | copy-start | bytes 6148
  195.8 76.5 %copy-start.19 = (f32[1024]{0:T(1024)S(1)}, f32[1024]{0:T(1024)}, u32[]{:S(2)}) copy-start(f32[1024]{0:T(1024)} %param.29) | copy-start | bytes 12292
  328.7 24.4 %copy-start.2 = (bf16[2048,768]{1,0:T(8,128)(2,1)S(1)}, bf16[2048,768]{1,0:T(8,128)(2,1)}, u32[]{:S(2)}) copy-start(bf16[2048,768]{1,0:T(8,128)(2,1)} %all-gather.11.cloned.1.call-done) | copy-start | bytes 9437188
  328.7 24.4 %copy-start.8 = (f32[4,1,512]{2,1,0:T(1,128)S(1)}, f32[4,1,512]{2,1,0:T(1,128)}, u32[]{:S(2)}) copy-start(f32[4,1,512]{2,1,0:T(1,128)} %all-gather) | copy-start | bytes 24580
  368.5 67.3 %all-gather.21.cloned.1.call-start = ((), (), s32[]{:S(2)}) async-start(), calls=%async_computation.9 | async-start | bytes 3932160 | tf_op jit(solution)/shard_map/all_gather | solution.py:33
  407.1 179.9 %all-gather.23.cloned.1.call-start = ((), (), s32[]{:S(2)}) async-start(), calls=%async_computation.10 | async-start | bytes 10485760 | tf_op jit(solution)/shard_map/all_gather | solution.py:166
  411.1 325.3 %all-gather.25.cloned.1.call-start = ((), (), s32[]{:S(2)}) async-start(), calls=%async_computation.11 | async-start | bytes 10485760 | tf_op jit(solution)/shard_map/all_gather | solution.py:172
  415.0 321.4 %copy-start.17 = (f32[2048]{0:T(1024)S(1)}, f32[2048]{0:T(1024)}, u32[]{:S(2)}) copy-start(f32[2048]{0:T(1024)} %param.35) | copy-start | bytes 24580
  415.0 321.4 %copy-start.18 = (f32[2048]{0:T(1024)S(1)}, f32[2048]{0:T(1024)}, u32[]{:S(2)}) copy-start(f32[2048]{0:T(1024)} %param.23) | copy-start | bytes 24580
  415.0 378.1 %reduce-scatter.5.cloned.1.call-start = ((), (), s32[]{:S(2)}) async-start(), calls=%async_computation.12 | async-start | bytes 3932160 | tf_op jit(solution)/shard_map/reduce_scatter | solution.py:179
  435.8 300.6 %copy-start.3 = (bf16[2048,768]{0,1:T(8,128)(2,1)S(1)}, bf16[2048,768]{0,1:T(8,128)(2,1)}, u32[]{:S(2)}) copy-start(bf16[2048,768]{0,1:T(8,128)(2,1)} %all-gather.21.cloned.1.call-done) | copy-start | bytes 9437188
  757.0 36.1 %copy-start.1 = (bf16[512,768]{0,1:T(8,128)(2,1)S(1)}, bf16[512,768]{0,1:T(8,128)(2,1)}, u32[]{:S(2)}) copy-start(bf16[512,768]{0,1:T(8,128)(2,1)} %add_convert_fusion.1) | copy-start | bytes 2359300
  (10 other events, 96.3 us)
Sparse Core Ops, SparseCore 0:
  8.9 31.2 all-gather.10
  41.7 83.7 all-gather.12
  127.1 64.1 all-gather.16
  192.8 79.5 all-gather.14
  273.8 79.2 all-gather.18
  368.6 36.1 reduce-scatter.2
  407.2 28.4 all-gather.20
  437.3 149.6 all-gather.22
  588.6 147.7 all-gather.24
  757.1 35.8 reduce-scatter.4
